TPU v7x, 32 devices: a whole 2x2x4 slice. The times are simulated.
32 devices in a mesh: sp: 4 (over z), fs: 4 (over y, x), tp: 2 (over core).
Axes of the slice: x: 2, y: 2, z: 4, core: 2. Of those that a mesh axis runs over, the one named last changes fastest.
Arguments:
- tokens: bfloat16 [2048, 2048], P(('fs', 'sp'), 'tp'), parts along dimension 0, may hold values from -6 to 6
- norm_gain: float32 [2048], replicated, may hold values from 0.1 to 1.9
- w_recur_in: bfloat16 [2048, 1024], P(None, 'tp'), may hold values from -0.125 to 0.125
- conv_weight: float32 [4, 1024], P(None, 'tp'), may hold values from -3 to 3
- w_gate_decay: bfloat16 [16, 64, 64], P('tp'), may hold values from -0.75 to 0.75
- w_gate_input: bfloat16 [16, 64, 64], P('tp'), may hold values from -0.75 to 0.75
- decay_base: float32 [1024], P('tp'), may hold values from 0 to 0.01, as said below
- extra_decay: float32 [2048, 16], P(('fs', 'sp'), 'tp'), parts along dimension 0, may hold values from 0 to 1, as said below
- w_query: bfloat16 [2048, 1024], P(None, 'tp'), may hold values from -1 to 1
- w_key: bfloat16 [2048, 256], P(None, 'tp'), may hold values from -20 to 20
- w_value: bfloat16 [2048, 256], P(None, 'tp'), may hold values from -0.125 to 0.125
- mix_lambda: float32 [8], P('tp'), may hold values from 0.3 to 0.8
- head_gain: float32 [128], replicated, may hold values from 0.1 to 1.9
- w_out_recur: bfloat16 [1024, 2048], P('tp'), may hold values from -0.125 to 0.125
- w_out_attend: bfloat16 [1024, 2048], P('tp'), may hold values from -0.125 to 0.125
- out_gain: float32 [2048], replicated, may hold values from 0.1 to 1.9
Outputs:
- mixed: bfloat16 [2048, 2048], P(('fs', 'sp', 'tp')), parts along dimension 0
There are 4 independent parts, one for each index of `fs`. A program takes and returns all parts, laid end to end along the dimension named above; an argument that names none is the same for every part. Nothing has to cross between parts.
Inputs may be any that keep to these rules, and one draw needn't show every extreme that they name: `decay_base`: positive rates of each channel. `extra_decay`: non-negative added log-decays.
All inputs are finite; a program needn't handle non-finite values.
Results may differ from a plain program's by a relative error of at most 0.012.
The roundings to bfloat16 on the way count: a program that leaves them out, or rounds other values in their place, can miss the bound.
Values may be sent and summed in bfloat16 or wider, within the bound.
A program may use at most 128 MiB of HBM per device.

v0:
```python
import jax
import jax.numpy as jnp
from jax import lax
from jax.sharding import PartitionSpec as P

D = 2048
HEAD = 64
DV = 128
lru_rate = 8.0
norm_eps = 1e-06


def shifted(block, axis, distance):
    devices = range(lax.axis_size(axis))
    route = [(i - distance, i) for i in devices if i - distance in devices]
    return lax.ppermute(block, axis, route)


def prefix(part, axis, combine, identity):
    place = lax.axis_index(axis)
    gathered = jax.tree.map(lambda a: lax.all_gather(a, axis), part)
    state = jax.tree.map(lambda a, e: jnp.zeros_like(a) + jnp.asarray(e, a.dtype), part, identity)

    def one(lap, state):
        return combine(
            state, jax.tree.map(lambda a: lax.dynamic_index_in_dim(a, lap, 0, False), gathered)
        )

    return lax.fori_loop(0, place, one, state)


def chain(earlier, later):
    return (earlier[0] * later[0], later[0] * earlier[1] + later[1])


def body(
    tokens,
    norm_gain,
    w_recur_in,
    conv_weight,
    w_gate_decay,
    w_gate_input,
    decay_base,
    extra_decay,
    w_query,
    w_key,
    w_value,
    mix_lambda,
    head_gain,
    w_out_recur,
    w_out_attend,
    out_gain,
):
    row_count = tokens.shape[0]
    recur_cols = w_recur_in.shape[1]
    query_cols = w_query.shape[1]
    key_cols = w_key.shape[1]
    all_weights = jnp.concatenate([w_recur_in, w_query, w_key, w_value], axis=1)
    wide_piece = lax.all_gather(tokens, "tp", axis=1, tiled=True).astype(jnp.float32)
    scaled = (wide_piece * norm_gain).astype(jnp.bfloat16)
    accum = jnp.dot(scaled, all_weights, preferred_element_type=jnp.float32)
    squares = jnp.sum(wide_piece * wide_piece, axis=1, keepdims=True)
    accum, squares = (accum, squares)
    inverse = lax.rsqrt(squares / D + norm_eps)
    projected = (accum * inverse).astype(jnp.bfloat16)
    recur_in = projected[:, :recur_cols]
    queries = projected[:, recur_cols : recur_cols + query_cols]
    keys = projected[:, recur_cols + query_cols : recur_cols + query_cols + key_cols]
    values = projected[:, recur_cols + query_cols + key_cols :]
    taps = conv_weight.shape[0]
    carried_rows = shifted(recur_in[row_count - (taps - 1) :], "sp", 1)
    padded = jnp.concatenate([carried_rows, recur_in], axis=0).astype(jnp.float32)
    conv_acc = jnp.zeros((row_count, recur_cols), jnp.float32)
    for offset in range(taps):
        conv_acc = conv_acc + conv_weight[offset] * padded[offset : offset + row_count]
    conv_in = conv_acc.astype(jnp.bfloat16)
    gate_blocks = w_gate_decay.shape[0]
    blocks = conv_in.reshape(row_count, gate_blocks, HEAD)
    decay_gate = jax.nn.sigmoid(
        jnp.einsum("thi,hij->thj", blocks, w_gate_decay, preferred_element_type=jnp.float32)
    ).reshape(row_count, recur_cols)
    input_gate = jax.nn.sigmoid(
        jnp.einsum("thi,hij->thj", blocks, w_gate_input, preferred_element_type=jnp.float32)
    ).reshape(row_count, recur_cols)
    log_decay = -lru_rate * decay_gate * decay_base - jnp.repeat(extra_decay, HEAD, axis=1)
    decay = jnp.exp(log_decay)
    inject = jnp.sqrt(-jnp.expm1(2.0 * log_decay)) * input_gate * conv_in.astype(jnp.float32)
    decay_cum, local_state = lax.associative_scan(chain, (decay, inject), axis=0)
    identity = (jnp.ones((recur_cols,), jnp.float32), jnp.zeros((recur_cols,), jnp.float32))
    carried = prefix((decay_cum[row_count - 1], local_state[row_count - 1]), "sp", chain, identity)
    recur_out = (local_state + decay_cum * carried[1]).astype(jnp.bfloat16)
    kv_local = key_cols // (2 * HEAD)
    heads_local = query_cols // (2 * HEAD)
    group_size = heads_local // kv_local
    local_query = queries.reshape(row_count, kv_local, group_size, 2, HEAD)
    offset_rows = lax.axis_index("sp") * row_count
    positions = offset_rows + jnp.arange(row_count, dtype=jnp.int32)
    last_position = offset_rows + row_count - 1
    lambdas = mix_lambda.reshape(kv_local, group_size)
    start_state = (
        jnp.full((2, kv_local, group_size, row_count), -1e30, jnp.float32),
        jnp.zeros((2, kv_local, group_size, row_count), jnp.float32),
        jnp.zeros((2, row_count, kv_local, group_size, DV), jnp.float32),
    )
    key_piece = lax.all_gather(keys, "sp", axis=0, tiled=True)
    value_piece = lax.all_gather(values, "sp", axis=0, tiled=True)
    count = key_piece.shape[0]

    def update(state):
        peaks, totals, attends = state
        key_three = key_piece.reshape(count, kv_local, 2, HEAD)
        value_three = value_piece.reshape(count, kv_local, DV)
        allowed = positions[:, None] >= jnp.arange(count, dtype=jnp.int32)[None, :]
        new_peaks, new_totals, new_attends = ([], [], [])
        for mapping in range(2):
            scores = jnp.einsum(
                "bkgd,tkd->kgbt",
                local_query[:, :, :, mapping, :],
                key_three[:, :, mapping, :],
                preferred_element_type=jnp.float32,
            ) * HEAD ** (-0.5)
            scores = jnp.where(allowed, scores, -jnp.inf)
            peak = jnp.maximum(peaks[mapping], jnp.max(scores, axis=-1))
            correction = jnp.exp(peaks[mapping] - peak)
            expo = jnp.exp(scores - peak[..., None])
            new_totals.append(totals[mapping] * correction + jnp.sum(expo, axis=-1))
            gained = jnp.einsum(
                "kgbt,tke->bkge",
                expo.astype(jnp.bfloat16),
                value_three,
                preferred_element_type=jnp.float32,
            )
            new_attends.append(
                attends[mapping] * jnp.transpose(correction, (2, 0, 1))[..., None] + gained
            )
            new_peaks.append(peak)
        return (jnp.stack(new_peaks), jnp.stack(new_totals), jnp.stack(new_attends))

    peaks, totals, attends = lax.cond(
        jnp.int32(0) <= last_position, update, lambda state: state, start_state
    )
    first = attends[0] / jnp.transpose(totals[0], (2, 0, 1))[..., None]
    second = attends[1] / jnp.transpose(totals[1], (2, 0, 1))[..., None]
    head_out = (first - lambdas[None, :, :, None] * second).reshape(row_count, heads_local, DV)
    normed = (
        head_out
        * lax.rsqrt(jnp.mean(head_out * head_out, axis=-1, keepdims=True) + norm_eps)
        * head_gain
    )
    attend_out = normed.astype(jnp.bfloat16).reshape(row_count, heads_local * DV)
    recur_rows, attend_rows = (
        lax.all_to_all(recur_out, "tp", split_axis=0, concat_axis=1, tiled=True),
        lax.all_to_all(attend_out, "tp", split_axis=0, concat_axis=1, tiled=True),
    )
    whole_recur, whole_attend = (
        lax.all_gather(w_out_recur, "tp", axis=0, tiled=True),
        lax.all_gather(w_out_attend, "tp", axis=0, tiled=True),
    )
    merged = jnp.dot(recur_rows, whole_recur, preferred_element_type=jnp.float32) + jnp.dot(
        attend_rows, whole_attend, preferred_element_type=jnp.float32
    )
    final = (
        merged * lax.rsqrt(jnp.mean(merged * merged, axis=1, keepdims=True) + norm_eps) * out_gain
    )
    return final.astype(jnp.bfloat16)


def solution(mesh):
    in_specs = (
        P(("fs", "sp"), "tp"),
        P(),
        P(None, "tp"),
        P(None, "tp"),
        P("tp", None, None),
        P("tp", None, None),
        P("tp"),
        P(("fs", "sp"), "tp"),
        P(None, "tp"),
        P(None, "tp"),
        P(None, "tp"),
        P("tp"),
        P(),
        P("tp", None),
        P("tp", None),
        P(),
    )
    out_specs = P(("fs", "sp", "tp"), None)
    return jax.shard_map(body, mesh=mesh, in_specs=in_specs, out_specs=out_specs, check_vma=False)
```

profile of v0, /device:TPU:0, one launch (start us, length us, event | category | flops | bytes accessed | tf_op | source)
XLA Modules:
  0.0 101.6 jit_solution(12139623973826426824)
XLA Ops:
  6.5 0.7 all-gather.5.cloned.1.call-update
  7.3 2.5 %all_gather.21 = bf16[128,2048]{1,0:T(8,128)(2,1)S(1)} all-gather(bf16[128,1024]{1,0:T(8,128)(2,1)} %param.20), channel_id=1, replica_groups=mesh['sp'=4,'fs'=4,'tp'=2] {'tp'}, dimensions={1}, use_global_device_ids=true | all-gather | bytes 786432 | tf_op jit(solution)/shard_map/all_gather | solution.py:59
  9.8 0.2 fusion.43
  10.0 3.2 %fusion.33 = bf16[128,1280]{1,0:T(8,128)(2,1)S(1)} fusion(bf16[2048,128]{1,0:T(8,128)(2,1)} %param.30, bf16[2048,128]{1,0:T(8,128)(2,1)} %param.29, bf16[2048,512]{1,0:T(8,128)(2,1)} %param.28, bf16[2048,512]{1,0:T(8,128)(2,1)} %param.22, bf16[128,2048]{1,0:T(8,128)(2,1)S(1)} %all_gather.21, f32[2048]{0:T(1024)} %param.21, f32[128]{0:T(128)S(1)} %add_rsqrt_fusion.2), kind=kOutput, calls=%fused_computation.52 | convolution fusion | flops 693174272 | bytes 6103552 | tf_op jit(solution)/shard_map/dot_general | solution.py:61
  13.2 4.8 %collective-permute-start = (bf16[3,512]{1,0:T(4,128)(2,1)S(1)}, bf16[3,512]{1,0:T(4,128)(2,1)S(1)}, u32[]{:S(2)}, u32[]{:S(2)}) collective-permute-start(bf16[3,512]{1,0:T(4,128)(2,1)S(1)} %slice.358), channel_id=1, source_target_pairs={{0,8},{8,16},{16,24},{1,9},{9,17},{17,25},{2,10},{10,18},{18,26},{... | collective-permute-start | bytes 9224 | tf_op jit(solution)/shard_map/ppermute | solution.py:16
  18.0 13.6 %all_gather.25 = bf16[512,128]{1,0:T(8,128)(2,1)S(1)} all-gather(bf16[128,128]{1,0:T(8,128)(2,1)S(1)} %get-tuple-element.115), channel_id=1, replica_groups=mesh['sp'=4,'fs'=4,'tp'=2] {'sp'}, dimensions={0}, use_global_device_ids=true | all-gather | bytes 163840 | tf_op jit(solution)/shard_map/all_gather | solution.py:105
  31.6 13.4 %all_gather.26 = bf16[512,128]{1,0:T(8,128)(2,1)S(1)} all-gather(bf16[128,128]{1,0:T(8,128)(2,1)S(1)} %get-tuple-element.114), channel_id=1, replica_groups=mesh['sp'=4,'fs'=4,'tp'=2] {'sp'}, dimensions={0}, use_global_device_ids=true | all-gather | bytes 163840 | tf_op jit(solution)/shard_map/all_gather | solution.py:106
  45.0 2.2 %conditional.1 = (f32[2,1,4,128]{3,2,1,0:T(4,128)S(1)}, f32[2,128,1,4,128]{4,1,3,2,0:T(8,128)S(1)}) conditional(s32[]{:T(128)} %convert_element_type.45, () %tuple.21, (s32[]{:T(128)}, s32[128]{0:T(128)S(1)}, bf16[512,128]{1,0:T(8,128)(2,1)S(1)}, bf16[128,1280]{1,0:T(8,128)(2,1)S(1)}, bf16[512,128]{1,0:T(8,128)(2,1)S(1)}) %tuple.22), branch_computations={%region_3.4_spmd, %region_4.9_spmd} | conditional | flops 205328512 | bytes 9819668 | solution.py:139
  45.0 0.2 copy.57
  45.3 0.1 copy.56
  45.4 0.3 fusion.65
  45.8 0.2 fusion.11
  46.0 0.3 fusion.66
  46.3 0.2 fusion.9
  46.5 0.4 fusion.5
  46.9 0.4 fusion.7
  47.3 0.1 copy.72
  47.4 0.1 copy.73
  47.5 0.3 fusion.53
  47.9 0.1 copy.62
  48.0 0.2 mul.337
  48.2 0.1 mul.338
  48.4 0.2 copy.58
  48.7 0.2 copy.60
  49.0 0.2 div.75.clone
  49.2 0.1 div.76
  49.3 0.2 div.79.clone
  49.5 0.1 div.80
  49.7 0.8 multiply_convert_fusion.1
  50.5 3.4 %all-to-all-start.1 = ((bf16[2,64,512]{2,1,0:T(8,128)(2,1)}), bf16[2,64,512]{2,1,0:T(8,128)(2,1)S(1)}, u32[]{:S(2)}, u32[]{:S(2)}) async-start(bf16[2,64,512]{2,1,0:T(8,128)(2,1)} %multiply_convert_fusion.1), calls=%async_computation.1 | async-start | bytes 262144 | tf_op jit(solution)/shard_map/all_to_all | solution.py:153
  53.9 0.7 all-gather.7.cloned.1.call-update
  54.7 0.1 copy.52
  54.8 0.5 all-to-all-done.1
  55.4 0.1 fusion.47
  55.5 0.1 copy.49
  55.6 0.3 fusion.41
  55.9 0.1 copy.51
  56.0 0.3 fusion.38
  56.3 0.1 copy.54
  56.5 0.3 convert_multiply_fusion.2
  58.2 0.2 slice.282
  58.4 0.2 slice.331
  59.6 11.9 %all-gather.1 = f32[4,1,512]{2,1,0:T(1,128)S(1)} all-gather(f32[1,1,512]{2,1,0:T(1,128)S(1)} %add_bitcast_fusion.2), channel_id=1, replica_groups=mesh['sp'=4,'fs'=4,'tp'=2] {'sp'}, dimensions={0}, use_global_device_ids=true | all-gather | bytes 10240 | tf_op jit(solution)/shard_map/all_gather | solution.py:21
  71.7 11.9 %all-gather = f32[4,1,512]{2,1,0:T(1,128)S(1)} all-gather(f32[1,1,512]{2,1,0:T(1,128)S(1)} %add_bitcast_fusion.3), channel_id=1, replica_groups=mesh['sp'=4,'fs'=4,'tp'=2] {'sp'}, dimensions={0}, use_global_device_ids=true | all-gather | bytes 10240 | tf_op jit(solution)/shard_map/all_gather | solution.py:21
  83.8 3.8 %all_to_all.35 = bf16[2,64,512]{2,1,0:T(8,128)(2,1)S(1)} all-to-all(bf16[2,64,512]{2,1,0:T(8,128)(2,1)S(1)} %bitcast.174), channel_id=1, replica_groups=mesh['sp'=4,'fs'=4,'tp'=2] {'tp'}, dimensions={0} | all-to-all | bytes 262144 | tf_op jit(solution)/shard_map/all_to_all | solution.py:152
  87.6 3.0 %fusion.71 = f32[64,2048]{1,0:T(8,128)S(1)} fusion(bf16[64,1024]{1,0:T(8,128)(2,1)S(1)} %bitcast.175, bf16[1024,2048]{1,0:T(8,128)(2,1)} %all-gather.5.cloned.1.call-done), kind=kOutput, calls=%fused_computation.154 | convolution fusion | flops 268435456 | bytes 4849664 | tf_op jit(solution)/shard_map/dot_general | solution.py:159
  90.7 3.2 %multiply_reduce_fusion = (f32[64]{0:T(128)S(1)}, f32[64,2048]{1,0:T(8,128)S(1)}) fusion(f32[64,2048]{1,0:T(8,128)S(1)} %fusion.71, bf16[64,1024]{1,0:T(8,128)(2,1)S(1)} %bitcast.173, bf16[1024,2048]{1,0:T(8,128)(2,1)} %all-gather.7.cloned.1.call-done), kind=kOutput, calls=%fused_computation.67 | convolution fusion | flops 268828608 | bytes 5374208 | tf_op jit(solution)/shard_map/dot_general | solution.py:159
  93.9 0.8 multiply_convert_fusion
  (155 shorter events, 2.8 us)
Async XLA Ops:
  6.5 49.1 %copy-start = (bf16[8,64,64]{2,1,0:T(8,128)(2,1)S(1)}, bf16[8,64,64]{2,1,0:T(8,128)(2,1)}, u32[]{:S(2)}) copy-start(bf16[8,64,64]{2,1,0:T(8,128)(2,1)} %param.24) | copy-start | bytes 196612
  6.5 81.1 %all-gather.5.cloned.1.call-start = ((), (), s32[]{:S(2)}) async-start(), calls=%async_computation.2 | async-start | bytes 6291456 | tf_op jit(solution)/shard_map/all_gather | solution.py:156
  13.2 42.1 %collective-permute-start = (bf16[3,512]{1,0:T(4,128)(2,1)S(1)}, bf16[3,512]{1,0:T(4,128)(2,1)S(1)}, u32[]{:S(2)}, u32[]{:S(2)}) collective-permute-start(bf16[3,512]{1,0:T(4,128)(2,1)S(1)} %slice.358), channel_id=1, source_target_pairs={{0,8},{8,16},{16,24},{1,9},{9,17},{17,25},{2,10},{10,18},{18,26},{... | collective-permute-start | bytes 9224 | tf_op jit(solution)/shard_map/ppermute | solution.py:16
  45.0 2.5 %copy-start.4 = (f32[4]{0:T(128)S(1)}, f32[4]{0:T(128)}, u32[]{:S(2)}) copy-start(f32[4]{0:T(128)} %param.31) | copy-start | bytes 52
  47.3 2.3 %copy-start.6 = (f32[128]{0:T(128)S(1)}, f32[128]{0:T(128)}, u32[]{:S(2)}) copy-start(f32[128]{0:T(128)} %param.32) | copy-start | bytes 1540
  48.3 6.3 %copy-start.2 = (f32[4,512]{1,0:T(4,128)S(1)}, f32[4,512]{1,0:T(4,128)}, u32[]{:S(2)}) copy-start(f32[4,512]{1,0:T(4,128)} %param.23) | copy-start | bytes 24580
  48.3 6.3 %copy-start.5 = (f32[512]{0:T(512)S(1)}, f32[512]{0:T(512)}, u32[]{:S(2)}) copy-start(f32[512]{0:T(512)} %param.26) | copy-start | bytes 6148
  48.4 6.3 %copy-start.3 = (f32[128,8]{0,1:T(8,128)S(1)}, f32[128,8]{0,1:T(8,128)}, u32[]{:S(2)}) copy-start(f32[128,8]{0,1:T(8,128)} %param.27) | copy-start | bytes 12292
  49.7 6.4 %copy-start.7 = (bf16[8,64,64]{2,1,0:T(8,128)(2,1)S(1)}, bf16[8,64,64]{2,1,0:T(8,128)(2,1)}, u32[]{:S(2)}) copy-start(bf16[8,64,64]{2,1,0:T(8,128)(2,1)} %param.25) | copy-start | bytes 196612
  50.5 4.8 %all-to-all-start.1 = ((bf16[2,64,512]{2,1,0:T(8,128)(2,1)}), bf16[2,64,512]{2,1,0:T(8,128)(2,1)S(1)}, u32[]{:S(2)}, u32[]{:S(2)}) async-start(bf16[2,64,512]{2,1,0:T(8,128)(2,1)} %multiply_convert_fusion.1), calls=%async_computation.1 | async-start | bytes 262144 | tf_op jit(solution)/shard_map/all_to_all | solution.py:153
  53.8 36.9 %all-gather.7.cloned.1.call-start = ((), (), s32[]{:S(2)}) async-start(), calls=%async_computation.3 | async-start | bytes 6291456 | tf_op jit(solution)/shard_map/all_gather | solution.py:157
  87.6 6.3 %copy-start.1 = (f32[2048]{0:T(1024)S(1)}, f32[2048]{0:T(1024)}, u32[]{:S(2)}) copy-start(f32[2048]{0:T(1024)} %param.35) | copy-start | bytes 24580
Sparse Core Ops, SparseCore 0:
  8.9 16.3 all-gather.4
  56.2 12.8 all-gather.6
where the time goes:
time: 102 us
  blocking collectives  57.2 us (56%)
  between operations  14.4 us (14%)
  matrix products  11.3 us (11%)
  starting transfers between devices  8.26 us (8%)
  local copies, waits for them, and re-layouts  4.75 us (5%)
  other arithmetic  3.69 us (4%)
  waiting for transfers between devices  1.91 us (2%)
    all_gather x2, blocking collectives, prefix(): gathered = jax.tree.map(lambda a: lax.all_gather(a, axis), part)  23.9 us
    all_gather x1, blocking collectives, body(): key_piece = lax.all_gather(keys, 'sp', axis=0, tiled=True)  13.6 us
    all_gather x1, blocking collectives, body(): value_piece = lax.all_gather(values, 'sp', axis=0, tiled=True)  13.4 us
    ppermute x1, starting transfers between devices, shifted(): return lax.ppermute(block, axis, route)  4.84 us
    all_to_all x1, blocking collectives, body(): lax.all_to_all(recur_out, 'tp', split_axis=0, concat_axis=1, tiled=True)  3.84 us
    all_to_all x1, starting transfers between devices, body(): lax.all_to_all(attend_out, 'tp', split_axis=0, concat_axis=1, tiled=True)  3.38 us
    dot_general x1, matrix products, body(): accum = jnp.dot(scaled, all_weights, preferred_element_type=jnp.float32)  3.19 us
    dot_general x1, matrix products, body(): jnp.dot(attend_rows, whole_attend, preferred_element_type=jnp.float32)  3.16 us
  transfers between devices with their start and end apart: 4, of which 1 were waited for; matrix products, arithmetic and copies ran while one was open for 15% of the time, Pallas kernels for 0%

commit v1 on v0

--- a/solution.py
+++ b/solution.py
@@ -2,12 +2,29 @@
 import jax.numpy as jnp
 from jax import lax
 from jax.sharding import PartitionSpec as P
+from jax.lax import axis_index, ppermute, psum
 
 D = 2048
 HEAD = 64
 DV = 128
 lru_rate = 8.0
 norm_eps = 1e-06
+
+
+def answer_layers_all_here(x_part, which_dim):
+    cores_n = psum(1, "sp")
+    e_next = sorted(((ix, (ix + 1) % cores_n) for ix in range(cores_n)))
+    x_next = x_part
+    pool = [x_next]
+    dd = 1
+    while dd < cores_n:
+        x_next = ppermute(x_next, "sp", e_next)
+        pool.insert(0, x_next)
+        dd = dd + 1
+    u1 = jnp.concatenate(pool, which_dim)
+    h_now = axis_index("sp") + 1
+    carry_out = jnp.roll(u1, h_now * x_part.shape[which_dim], which_dim)
+    return carry_out
 
 
 def shifted(block, axis, distance):
@@ -102,7 +119,7 @@
         jnp.zeros((2, kv_local, group_size, row_count), jnp.float32),
         jnp.zeros((2, row_count, kv_local, group_size, DV), jnp.float32),
     )
-    key_piece = lax.all_gather(keys, "sp", axis=0, tiled=True)
+    key_piece = answer_layers_all_here(keys, 0)
     value_piece = lax.all_gather(values, "sp", axis=0, tiled=True)
     count = key_piece.shape[0]
 

time: 102 us -> 98.2 us (0.963)
  blocking collectives: 57.2 us -> 48.3 us
  waiting for transfers between devices: 1.91 us -> 9.16 us
  starting transfers between devices: 8.26 us -> 6.55 us
    all_gather x1 -> x0, blocking collectives: 13.6 us -> none  [body(): key_piece = lax.all_gather(keys, 'sp', axis=0, tiled=True)]
    ppermute x0 -> x3, waiting for transfers between devices: none -> 7.42 us  [answer_layers_all_here(): x_next = ppermute(x_next, 'sp', e_next)]
    all_to_all x0 -> x1, blocking collectives: none -> 3.84 us  [body(): lax.all_to_all(attend_out, 'tp', split_axis=0, concat_axis=1, tiled=True)]
    all_to_all x1 -> x0, starting transfers between devices: 3.38 us -> none  [body(): lax.all_to_all(attend_out, 'tp', split_axis=0, concat_axis=1, tiled=True)]
    ppermute x0 -> x3, starting transfers between devices: none -> 3.04 us  [answer_layers_all_here(): x_next = ppermute(x_next, 'sp', e_next)]
    ppermute x1, starting transfers between devices: 4.84 us -> 3.47 us  [shifted(): return lax.ppermute(block, axis, route)]
  transfers between devices with their start and end apart: 4 -> 6, of which waited for: 1 -> 3; matrix products, arithmetic and copies ran while one was open for 15% -> 16% of each run, Pallas kernels for 0% -> 0%
where the time goes in v1:
time: 98.2 us; the launch traced here: 97.9 us
  blocking collectives  48.3 us (49%)
  between operations  14.4 us (15%)
  matrix products  11.3 us (12%)
  waiting for transfers between devices  9.16 us (9%)
  starting transfers between devices  6.55 us (7%)
  local copies, waits for them, and re-layouts  4.98 us (5%)
  other arithmetic  3.04 us (3%)
    all_gather x2, blocking collectives, prefix(): gathered = jax.tree.map(lambda a: lax.all_gather(a, axis), part)  24.8 us
    all_gather x1, blocking collectives, body(): value_piece = lax.all_gather(values, 'sp', axis=0, tiled=True)  13.3 us
    ppermute x3, waiting for transfers between devices, answer_layers_all_here(): x_next = ppermute(x_next, 'sp', e_next)  7.42 us
    all_to_all x1, blocking collectives, body(): lax.all_to_all(recur_out, 'tp', split_axis=0, concat_axis=1, tiled=True)  3.84 us
    all_to_all x1, blocking collectives, body(): lax.all_to_all(attend_out, 'tp', split_axis=0, concat_axis=1, tiled=True)  3.84 us
    ppermute x1, starting transfers between devices, shifted(): return lax.ppermute(block, axis, route)  3.47 us
    dot_general x1, matrix products, body(): accum = jnp.dot(scaled, all_weights, preferred_element_type=jnp.float32)  3.19 us
    dot_general x1, matrix products, body(): jnp.dot(attend_rows, whole_attend, preferred_element_type=jnp.float32)  3.16 us
  transfers between devices with their start and end apart: 6, of which 3 were waited for; matrix products, arithmetic and copies ran while one was open for 16% of the time, Pallas kernels for 0%

profile of v1, /device:TPU:0, one launch (start us, length us, event | category | flops | bytes accessed | tf_op | source)
XLA Modules:
  0.0 97.9 jit_solution(6308331883714014534)
XLA Ops:
  6.5 0.7 all-gather.5.cloned.1.call-update
  7.3 2.5 %all_gather.18 = bf16[128,2048]{1,0:T(8,128)(2,1)S(1)} all-gather(bf16[128,1024]{1,0:T(8,128)(2,1)} %param.20), channel_id=1, replica_groups=mesh['sp'=4,'fs'=4,'tp'=2] {'tp'}, dimensions={1}, use_global_device_ids=true | all-gather | bytes 786432 | tf_op jit(solution)/shard_map/all_gather | solution.py:76
  9.8 0.2 fusion.43
  10.1 3.2 %fusion.33 = bf16[128,1280]{1,0:T(8,128)(2,1)S(1)} fusion(bf16[2048,128]{1,0:T(8,128)(2,1)} %param.30, bf16[2048,128]{1,0:T(8,128)(2,1)} %param.29, bf16[2048,512]{1,0:T(8,128)(2,1)} %param.28, bf16[2048,512]{1,0:T(8,128)(2,1)} %param.22, bf16[128,2048]{1,0:T(8,128)(2,1)S(1)} %all_gather.18, f32[2048]{0:T(1024)} %param.21, f32[128]{0:T(128)S(1)} %add_rsqrt_fusion.2), kind=kOutput, calls=%fused_computation.53 | convolution fusion | flops 693174272 | bytes 6103552 | tf_op jit(solution)/shard_map/dot_general | solution.py:78
  13.3 3.0 %collective-permute-start.1 = (bf16[128,128]{1,0:T(8,128)(2,1)S(1)}, bf16[128,128]{1,0:T(8,128)(2,1)S(1)}, u32[]{:S(2)}, u32[]{:S(2)}) collective-permute-start(bf16[128,128]{1,0:T(8,128)(2,1)S(1)} %slice.430), channel_id=1, source_target_pairs={{0,8},{8,16},{16,24},{24,0},{1,9},{9,17},{17,25},{25,1},{2,10},{10... | collective-permute-start | bytes 98312 | tf_op jit(solution)/shard_map/ppermute | solution.py:21
  16.3 3.5 %collective-permute-start = (bf16[3,512]{1,0:T(4,128)(2,1)S(1)}, bf16[3,512]{1,0:T(4,128)(2,1)S(1)}, u32[]{:S(2)}, u32[]{:S(2)}) collective-permute-start(bf16[3,512]{1,0:T(4,128)(2,1)S(1)} %slice.378), channel_id=1, source_target_pairs={{0,8},{8,16},{16,24},{1,9},{9,17},{17,25},{2,10},{10,18},{18,26},{... | collective-permute-start | bytes 9224 | tf_op jit(solution)/shard_map/ppermute | solution.py:33
  20.0 0.1 copy.52
  20.1 1.0 collective-permute-done
  21.1 0.1 fusion.47
  21.2 0.1 copy.49
  21.4 0.3 fusion.41
  21.7 0.1 copy.51
  21.8 0.3 fusion.38
  22.1 0.1 copy.54
  22.2 0.3 convert_multiply_fusion.2
  23.9 0.2 slice.297
  24.1 0.2 slice.346
  25.5 12.9 %all-gather.1 = f32[4,1,512]{2,1,0:T(1,128)S(1)} all-gather(f32[1,1,512]{2,1,0:T(1,128)S(1)} %add_bitcast_fusion.2), channel_id=1, replica_groups=mesh['sp'=4,'fs'=4,'tp'=2] {'sp'}, dimensions={0}, use_global_device_ids=true | all-gather | bytes 10240 | tf_op jit(solution)/shard_map/all_gather | solution.py:38
  38.4 11.9 %all-gather = f32[4,1,512]{2,1,0:T(1,128)S(1)} all-gather(f32[1,1,512]{2,1,0:T(1,128)S(1)} %add_bitcast_fusion.3), channel_id=1, replica_groups=mesh['sp'=4,'fs'=4,'tp'=2] {'sp'}, dimensions={0}, use_global_device_ids=true | all-gather | bytes 10240 | tf_op jit(solution)/shard_map/all_gather | solution.py:38
  50.4 5.7 %collective-permute-done.2 = bf16[128,128]{1,0:T(8,128)(2,1)S(1)} collective-permute-done((bf16[128,128]{1,0:T(8,128)(2,1)S(1)}, bf16[128,128]{1,0:T(8,128)(2,1)S(1)}, u32[]{:S(2)}, u32[]{:S(2)}) %collective-permute-start.2) | collective-permute-done | bytes 32800 | tf_op jit(solution)/shard_map/ppermute | solution.py:21
  56.2 3.8 %all_to_all.35 = bf16[2,64,512]{2,1,0:T(8,128)(2,1)S(1)} all-to-all(bf16[2,64,512]{2,1,0:T(8,128)(2,1)S(1)} %bitcast.175), channel_id=1, replica_groups=mesh['sp'=4,'fs'=4,'tp'=2] {'tp'}, dimensions={0} | all-to-all | bytes 262144 | tf_op jit(solution)/shard_map/all_to_all | solution.py:169
  60.0 1.7 %collective-permute-done.3 = bf16[128,128]{1,0:T(8,128)(2,1)S(1)} collective-permute-done((bf16[128,128]{1,0:T(8,128)(2,1)S(1)}, bf16[128,128]{1,0:T(8,128)(2,1)S(1)}, u32[]{:S(2)}, u32[]{:S(2)}) %collective-permute-start.3) | collective-permute-done | bytes 32800 | tf_op jit(solution)/shard_map/ppermute | solution.py:21
  61.9 13.3 %all_gather.22 = bf16[512,128]{1,0:T(8,128)(2,1)S(1)} all-gather(bf16[128,128]{1,0:T(8,128)(2,1)S(1)} %get-tuple-element.245), channel_id=1, replica_groups=mesh['sp'=4,'fs'=4,'tp'=2] {'sp'}, dimensions={0}, use_global_device_ids=true | all-gather | bytes 163840 | tf_op jit(solution)/shard_map/all_gather | solution.py:123
  75.2 2.4 %conditional.1 = (f32[2,1,4,128]{3,2,1,0:T(4,128)S(1)}, f32[2,128,1,4,128]{4,1,3,2,0:T(8,128)S(1)}) conditional(s32[]{:T(128)} %convert_element_type.51, () %tuple.32, (s32[]{:T(128)}, s32[128]{0:T(128)S(1)}, s32[]{:T(128)}, s32[]{:T(128)}, bf16[1024,128]{1,0:T(8,128)(2,1)S(1)}, /*index=5*/bf16[128,1280]{1,0:T(8,128)(2,1)S(1)}, ...), branch_computations={%region_3.4_spmd, %region_4.9_spmd.clone} | conditional | flops 205328528 | bytes 10344115 | solution.py:156
  75.2 0.1 copy.56
  75.4 0.1 constant_dynamic-slice_fusion.2
  75.5 0.2 copy.57
  75.8 0.3 fusion.65
  76.2 0.2 fusion.11
  76.3 0.3 fusion.66
  76.7 0.2 fusion.9
  76.9 0.4 fusion.5
  77.2 0.4 fusion.7
  77.7 0.1 copy.72
  77.8 0.1 copy.73
  77.9 0.3 fusion.53
  78.2 0.1 copy.62
  78.3 0.2 mul.347
  78.7 0.2 copy.58
  79.0 0.2 copy.60
  79.3 0.2 div.75.clone
  79.5 0.1 div.76
  79.6 0.2 div.79.clone
  79.9 0.1 multiply_convert_fusion.1
  80.1 3.8 %all_to_all.36 = bf16[2,64,512]{2,1,0:T(8,128)(2,1)S(1)} all-to-all(bf16[2,64,512]{2,1,0:T(8,128)(2,1)S(1)} %multiply_convert_fusion.1), channel_id=1, replica_groups=mesh['sp'=4,'fs'=4,'tp'=2] {'tp'}, dimensions={0} | all-to-all | bytes 262144 | tf_op jit(solution)/shard_map/all_to_all | solution.py:170
  84.0 3.0 %fusion.71 = f32[64,2048]{1,0:T(8,128)S(1)} fusion(bf16[64,1024]{1,0:T(8,128)(2,1)S(1)} %bitcast.173, bf16[1024,2048]{1,0:T(8,128)(2,1)} %all-gather.5.cloned.1.call-done), kind=kOutput, calls=%fused_computation.163 | convolution fusion | flops 268435456 | bytes 4849664 | tf_op jit(solution)/shard_map/dot_general | solution.py:176
  87.0 3.2 %multiply_reduce_fusion = (f32[64]{0:T(128)S(1)}, f32[64,2048]{1,0:T(8,128)S(1)}) fusion(f32[64,2048]{1,0:T(8,128)S(1)} %fusion.71, bf16[64,1024]{1,0:T(8,128)(2,1)S(1)} %bitcast.174, bf16[1024,2048]{1,0:T(8,128)(2,1)} %all-gather.7.cloned.1.call-done), kind=kOutput, calls=%fused_computation.68 | convolution fusion | flops 268828608 | bytes 5374208 | tf_op jit(solution)/shard_map/dot_general | solution.py:176
  90.2 0.8 multiply_convert_fusion
  (168 shorter events, 3.2 us)
Async XLA Ops:
  6.5 14.8 %copy-start = (bf16[8,64,64]{2,1,0:T(8,128)(2,1)S(1)}, bf16[8,64,64]{2,1,0:T(8,128)(2,1)}, u32[]{:S(2)}) copy-start(bf16[8,64,64]{2,1,0:T(8,128)(2,1)} %param.24) | copy-start | bytes 196612
  6.5 77.4 %all-gather.5.cloned.1.call-start = ((), (), s32[]{:S(2)}) async-start(), calls=%async_computation.2 | async-start | bytes 6291456 | tf_op jit(solution)/shard_map/all_gather | solution.py:173
  7.3 79.8 %all-gather.7.cloned.1.call-start = ((), (), s32[]{:S(2)}) async-start(), calls=%async_computation.3 | async-start | bytes 6291456 | tf_op jit(solution)/shard_map/all_gather | solution.py:174
  10.0 9.8 %copy-start.2 = (f32[4,512]{1,0:T(4,128)S(1)}, f32[4,512]{1,0:T(4,128)}, u32[]{:S(2)}) copy-start(f32[4,512]{1,0:T(4,128)} %param.23) | copy-start | bytes 24580
  10.0 9.8 %copy-start.4 = (f32[4]{0:T(128)S(1)}, f32[4]{0:T(128)}, u32[]{:S(2)}) copy-start(f32[4]{0:T(128)} %param.31) | copy-start | bytes 52
  10.0 9.8 %copy-start.6 = (f32[128]{0:T(128)S(1)}, f32[128]{0:T(128)}, u32[]{:S(2)}) copy-start(f32[128]{0:T(128)} %param.32) | copy-start | bytes 1540
  10.0 9.9 %copy-start.5 = (f32[512]{0:T(512)S(1)}, f32[512]{0:T(512)}, u32[]{:S(2)}) copy-start(f32[512]{0:T(512)} %param.26) | copy-start | bytes 6148
  10.1 9.9 %copy-start.3 = (f32[128,8]{0,1:T(8,128)S(1)}, f32[128,8]{0,1:T(8,128)}, u32[]{:S(2)}) copy-start(f32[128,8]{0,1:T(8,128)} %param.27) | copy-start | bytes 12292
  13.3 8.5 %copy-start.7 = (bf16[8,64,64]{2,1,0:T(8,128)(2,1)S(1)}, bf16[8,64,64]{2,1,0:T(8,128)(2,1)}, u32[]{:S(2)}) copy-start(bf16[8,64,64]{2,1,0:T(8,128)(2,1)} %param.25) | copy-start | bytes 196612
  13.3 37.0 %collective-permute-start.1 = (bf16[128,128]{1,0:T(8,128)(2,1)S(1)}, bf16[128,128]{1,0:T(8,128)(2,1)S(1)}, u32[]{:S(2)}, u32[]{:S(2)}) collective-permute-start(bf16[128,128]{1,0:T(8,128)(2,1)S(1)} %slice.430), channel_id=1, source_target_pairs={{0,8},{8,16},{16,24},{24,0},{1,9},{9,17},{17,25},{25,1},{2,10},{10... | collective-permute-start | bytes 98312 | tf_op jit(solution)/shard_map/ppermute | solution.py:21
  16.3 4.8 %collective-permute-start = (bf16[3,512]{1,0:T(4,128)(2,1)S(1)}, bf16[3,512]{1,0:T(4,128)(2,1)S(1)}, u32[]{:S(2)}, u32[]{:S(2)}) collective-permute-start(bf16[3,512]{1,0:T(4,128)(2,1)S(1)} %slice.378), channel_id=1, source_target_pairs={{0,8},{8,16},{16,24},{1,9},{9,17},{17,25},{2,10},{10,18},{18,26},{... | collective-permute-start | bytes 9224 | tf_op jit(solution)/shard_map/ppermute | solution.py:33
  50.3 5.8 %collective-permute-start.2 = (bf16[128,128]{1,0:T(8,128)(2,1)S(1)}, bf16[128,128]{1,0:T(8,128)(2,1)S(1)}, u32[]{:S(2)}, u32[]{:S(2)}) collective-permute-start(bf16[128,128]{1,0:T(8,128)(2,1)S(1)} %collective-permute-done.1), channel_id=1, source_target_pairs={{0,8},{8,16},{16,24},{24,0},{1,9},{9,17},{17,25},{25,1},{2,10},{10... | collective-permute-start | bytes 98312 | tf_op jit(solution)/shard_map/ppermute | solution.py:21
  56.1 5.7 %collective-permute-start.3 = (bf16[128,128]{1,0:T(8,128)(2,1)S(1)}, bf16[128,128]{1,0:T(8,128)(2,1)S(1)}, u32[]{:S(2)}, u32[]{:S(2)}) collective-permute-start(bf16[128,128]{1,0:T(8,128)(2,1)S(1)} %collective-permute-done.2), channel_id=1, source_target_pairs={{0,8},{8,16},{16,24},{24,0},{1,9},{9,17},{17,25},{25,1},{2,10},{10... | collective-permute-start | bytes 98312 | tf_op jit(solution)/shard_map/ppermute | solution.py:21
  83.9 6.3 %copy-start.1 = (f32[2048]{0:T(1024)S(1)}, f32[2048]{0:T(1024)}, u32[]{:S(2)}) copy-start(f32[2048]{0:T(1024)} %param.35) | copy-start | bytes 24580
Sparse Core Ops, SparseCore 0:
  8.9 16.3 all-gather.4
  26.8 14.8 all-gather.6
